TPU v7x, 32 devices: a whole 2x2x4 slice. The times are simulated.
32 devices in a mesh: sp: 16 (over z, y, x), tp: 2 (over core).
Axes of the slice: x: 2, y: 2, z: 4, core: 2. Of those that a mesh axis runs over, the one named last changes fastest.
Arguments:
- conv_value: bfloat16 [4096, 1024], P('sp', 'tp'), may hold values from -6 to 6
- conv_gate: bfloat16 [4096, 1024], P('sp', 'tp'), may hold values from -6 to 6
- taps: bfloat16 [31, 1024], P(None, 'tp'), may hold values from -1 to 1
- doc_ids: int32 [4096], P('sp'), may hold values from 0 to 3, never falling along the last dimension, each value on 1 to 2048 neighbouring positions
- gn_gain: float32 [1024], P('tp'), may hold values from 0.1 to 1.9
- gn_shift: float32 [1024], P('tp'), may hold values from -3 to 3
- conv_out: bfloat16 [1024, 2048], replicated, may hold values from -0.1875 to 0.1875
- residual: bfloat16 [4096, 2048], P(('sp', 'tp')), may hold values from -6 to 6
- norm_gain: float32 [2048], replicated, may hold values from 0.1 to 1.9
- routes: int32 [4096, 2], P(('sp', 'tp')), may hold values from 0 to 31, as said below
- route_weight: float32 [4096, 2], P(('sp', 'tp')), may hold values from 0.3 to 1.2
- expert_gate: bfloat16 [32, 2048, 512], P(('sp', 'tp')), may hold values from -0.125 to 0.125
- expert_up: bfloat16 [32, 2048, 512], P(('sp', 'tp')), may hold values from -0.125 to 0.125
- expert_down: bfloat16 [32, 512, 2048], P(('sp', 'tp')), may hold values from -0.25 to 0.25
- shared_gate: bfloat16 [2048, 512], replicated, may hold values from -0.125 to 0.125
- shared_up: bfloat16 [2048, 512], replicated, may hold values from -0.125 to 0.125
- shared_down: bfloat16 [512, 2048], replicated, may hold values from -0.25 to 0.25
Outputs:
- layer_out: bfloat16 [4096, 2048], P(('sp', 'tp'))
Inputs may be any that keep to these rules, and one draw needn't show every extreme that they name: `routes`: each row names 2 different experts. The rows of one device name each expert at most 16 times, and one expert, the same for every device, exactly 16 times. `doc_ids`: numbers never fall from one position to the next.
All inputs are finite; a program needn't handle non-finite values.
Results may differ from a plain program's by a relative error of at most 0.014.
Values may be sent and summed in bfloat16 or wider, within the bound.
A program may use at most 128 MiB of HBM per device.

v0:
```python
import jax
import jax.numpy as jnp
from jax import lax
from jax.sharding import PartitionSpec as P

GROUPS = 8


epsilon = 1e-06


def from_behind(x, axis, by):
    peers = lax.axis_size(axis)
    pairs = [(i, i + by) for i in range(peers) if 0 <= i + by < peers]
    return lax.ppermute(x, axis, pairs)


def per_device(
    conv_value,
    conv_gate,
    taps,
    doc_ids,
    gn_gain,
    gn_shift,
    conv_out,
    residual,
    norm_gain,
    routes,
    route_weight,
    expert_gate,
    expert_up,
    expert_down,
    shared_gate,
    shared_up,
    shared_down,
):
    position_count, channel_count = conv_value.shape
    kernel_width = taps.shape[0]
    model_width = residual.shape[1]
    glu_out = (
        conv_value.astype(jnp.float32) * jax.nn.sigmoid(conv_gate.astype(jnp.float32))
    ).astype(jnp.bfloat16)
    rim_start = position_count - kernel_width + 1
    edge_glu, edge_ids = from_behind((glu_out[rim_start:], doc_ids[rim_start:]), "sp", 1)
    longer_glu = jnp.concatenate([edge_glu, glu_out], axis=0)
    longer_ids = jnp.concatenate([edge_ids, doc_ids], axis=0)
    conv_sum = jnp.zeros((position_count, channel_count), jnp.float32)
    for offset in range(kernel_width):
        same_doc = (longer_ids[offset : offset + position_count] == doc_ids)[:, None]
        tap_term = taps[offset].astype(jnp.float32)[None, :] * longer_glu[
            offset : offset + position_count
        ].astype(jnp.float32)
        conv_sum = conv_sum + jnp.where(same_doc, tap_term, 0.0)
    core_split = lax.axis_size("tp")
    groups_here = GROUPS // core_split
    grouped = conv_sum.reshape(position_count, groups_here, channel_count // groups_here)
    group_mean = jnp.mean(grouped, axis=-1, keepdims=True)
    centered = grouped - group_mean
    group_var = jnp.mean(centered * centered, axis=-1, keepdims=True)
    normalized = (centered * lax.rsqrt(group_var + epsilon)).reshape(position_count, channel_count)
    conv_act = jax.nn.silu(normalized * gn_gain + gn_shift).astype(jnp.bfloat16)
    token_rows = lax.all_to_all(conv_act, "tp", split_axis=0, concat_axis=1, tiled=True)
    projected = jnp.dot(token_rows, conv_out, preferred_element_type=jnp.float32)
    stream = (residual.astype(jnp.float32) + projected).astype(jnp.bfloat16)
    stream_wide = stream.astype(jnp.float32)
    normed = (
        stream_wide
        * lax.rsqrt(jnp.mean(stream_wide * stream_wide, axis=-1, keepdims=True) + epsilon)
        * norm_gain
    ).astype(jnp.bfloat16)
    token_count, top_count = routes.shape
    sequence_split = lax.axis_size("sp")
    device_count = sequence_split * core_split
    local_experts = expert_gate.shape[0]
    experts = local_experts * device_count
    capacity = 2 * token_count * top_count // experts
    flat_routes = routes.reshape(-1)
    onehot = (flat_routes[:, None] == jnp.arange(experts, dtype=jnp.int32)[None, :]).astype(
        jnp.int32
    )
    slot_index = jnp.sum(jnp.cumsum(onehot, axis=0) * onehot, axis=1) - 1
    target = flat_routes * capacity + slot_index
    source = (
        jnp.full((experts * capacity,), token_count, jnp.int32)
        .at[target]
        .set(jnp.arange(token_count * top_count, dtype=jnp.int32) // top_count)
    )
    padded_rows = jnp.concatenate([normed, jnp.zeros((1, model_width), normed.dtype)], axis=0)
    outgoing = padded_rows[source]
    shared_hidden = (
        jax.nn.silu(jnp.dot(normed, shared_gate, preferred_element_type=jnp.float32))
        * jnp.dot(normed, shared_up, preferred_element_type=jnp.float32)
    ).astype(jnp.bfloat16)
    shared_out = jnp.dot(shared_hidden, shared_down, preferred_element_type=jnp.float32)
    parcel = outgoing.reshape(device_count, local_experts, capacity, model_width)
    arrived = lax.all_to_all(parcel, ("sp", "tp"), split_axis=0, concat_axis=0, tiled=True)
    expert_rows = arrived[:, 0].reshape(-1, model_width)
    gate_part = jnp.dot(expert_rows, expert_gate[0], preferred_element_type=jnp.float32)
    up_part = jnp.dot(expert_rows, expert_up[0], preferred_element_type=jnp.float32)
    hidden = (jax.nn.silu(gate_part) * up_part).astype(jnp.bfloat16)
    result = jnp.dot(hidden, expert_down[0], preferred_element_type=jnp.float32).astype(
        jnp.bfloat16
    )
    results = [result.reshape(arrived.shape[0], arrived.shape[2], model_width)]
    returned = lax.all_to_all(
        jnp.stack(results, axis=1), ("sp", "tp"), split_axis=0, concat_axis=0, tiled=True
    )
    picked = returned.reshape(experts * capacity, model_width)[target].reshape(
        token_count, top_count, model_width
    )
    routed = jnp.zeros((token_count, model_width), jnp.float32)
    for route_index in range(top_count):
        routed = routed + route_weight[:, route_index, None] * picked[:, route_index].astype(
            jnp.float32
        )
    return (stream_wide + shared_out + routed).astype(jnp.bfloat16)


def solution(mesh):
    return jax.shard_map(
        per_device,
        mesh=mesh,
        in_specs=(
            P("sp", "tp"),
            P("sp", "tp"),
            P(None, "tp"),
            P("sp"),
            P("tp"),
            P("tp"),
            P(),
            P(("sp", "tp"), None),
            P(),
            P(("sp", "tp"), None),
            P(("sp", "tp"), None),
            P(("sp", "tp"), None, None),
            P(("sp", "tp"), None, None),
            P(("sp", "tp"), None, None),
            P(),
            P(),
            P(),
        ),
        out_specs=P(("sp", "tp"), None),
        check_vma=False,
    )
```

profile of v0, /device:TPU:0, one launch (start us, length us, event | category | flops | bytes accessed | tf_op | source)
XLA Modules:
  0.0 168.0 jit_solution(8082973115691364182)
XLA Ops:
  0.0 0.0 copy-start
  0.0 0.9 slice.297
  0.9 4.9 %collective-permute-start = (s32[30]{0:T(128)S(1)}, s32[30]{0:T(128)S(1)}, u32[]{:S(2)}, u32[]{:S(2)}) collective-permute-start(s32[30]{0:T(128)S(1)} %slice.297), channel_id=1, source_target_pairs={{0,2},{2,4},{4,6},{6,8},{8,10},{10,12},{12,14},{14,16},{16,18},{18... | collective-permute-start | bytes 368 | tf_op jit(solution)/shard_map/ppermute | solution.py:15
  5.8 1.2 multiply_convert_fusion.2
  7.0 3.4 %collective-permute-start.1 = (bf16[30,512]{1,0:T(8,128)(2,1)S(1)}, bf16[30,512]{1,0:T(8,128)(2,1)S(1)}, u32[]{:S(2)}, u32[]{:S(2)}) collective-permute-start(bf16[30,512]{1,0:T(8,128)(2,1)S(1)} %slice.400), channel_id=1, source_target_pairs={{0,2},{2,4},{4,6},{6,8},{8,10},{10,12},{12,14},{14,16},{16,18},{18... | collective-permute-start | bytes 92168 | tf_op jit(solution)/shard_map/ppermute | solution.py:15
  10.4 1.0 slice_convert_fusion.30
  11.4 1.0 slice_convert_fusion.29
  12.4 0.8 copy.33
  13.2 0.1 eq.149
  13.3 0.1 eq.145
  13.5 0.7 broadcast_multiply_fusion.1
  14.2 0.6 reduce-window.6
  14.8 0.2 slice_reduce_fusion
  15.0 0.1 fusion.58
  15.1 0.1 copy.32
  15.2 0.1 mul.647
  15.4 1.4 scatter_custom_fusion
  16.8 0.0 collective-permute-done
  16.8 0.8 pad_add_fusion
  17.6 0.8 slice_compare_fusion.29
  18.4 0.8 slice_compare_fusion.28
  19.1 0.0 collective-permute-done.1
  19.1 4.0 %multiply_add_fusion = f32[256,512]{1,0:T(8,128)S(1)} fusion(bf16[256,512]{1,0:T(8,128)(2,1)S(1)} %multiply_convert_fusion.2, bf16[30,512]{1,0:T(8,128)(2,1)S(1)} %collective-permute-done.1, f32[512]{0:T(512)S(1)} %bitcast.151, f32[512]{0:T(512)S(1)} %bitcast.152, f32[512]{0:T(512)S(1)} %bitcast.123, f32[512]{0:T(512)S(1)} %bitcast.124, ...), kind=kLoop, calls=%fused_computation.62 | loop fusion | flops 27787264 | bytes 888320 | tf_op jit(solution)/shard_map/add | solution.py:53
  23.2 0.0 copy-start.6
  23.2 0.0 copy-start.7
  23.2 0.2 reshape.126
  23.4 0.3 reduce_sum.36
  23.8 0.6 multiply_reduce_fusion.1
  24.4 0.0 copy-start.4
  24.4 0.3 mul.630
  24.8 0.3 sub.25
  25.1 0.0 copy-done.6
  25.1 0.0 copy-done.7
  25.1 0.2 multiply_convert_fusion.1
  25.3 3.9 %all_to_all.29 = bf16[2,128,512]{2,1,0:T(8,128)(2,1)S(1)} all-to-all(bf16[2,128,512]{2,1,0:T(8,128)(2,1)S(1)} %bitcast.119), channel_id=1, replica_groups=mesh['sp'=16,'tp'=2] {'tp'}, dimensions={0} | all-to-all | bytes 524288 | tf_op jit(solution)/shard_map/all_to_all | solution.py:62
  29.3 0.2 copy.31
  29.5 0.0 copy-done.4
  29.5 0.0 copy-start.5
  29.5 3.0 %multiply_reduce_fusion = (f32[128]{0:T(128)S(1)}, f32[128,2048]{1,0:T(8,128)S(1)}) fusion(bf16[128,1024]{0,1:T(8,128)(2,1)S(1)} %bitcast.120, bf16[1024,2048]{1,0:T(8,128)(2,1)} %param.23, bf16[128,2048]{1,0:T(8,128)(2,1)S(1)} %copy-done.4), kind=kOutput, calls=%fused_computation.52 | convolution fusion | flops 538443648 | bytes 6029824 | tf_op jit(solution)/shard_map/dot_general | solution.py:63
  32.5 0.0 copy-start.2
  32.5 1.0 copy-done.2
  33.5 0.0 copy-done.5
  33.5 0.2 multiply_convert_fusion
  33.6 0.0 copy-start.1
  33.7 3.3 %gather_fusion = bf16[512,2048]{1,0:T(8,128)(2,1)} fusion(bf16[129,2048]{1,0:T(8,128)(2,1)S(1)} %concatenate.11, s32[1024]{0:T(1024)S(1)} %pad_clamp_fusion.1), kind=kCustom, calls=%fused_computation | custom fusion | bytes 4196352 | tf_op jit(solution)/shard_map/gather | solution.py:89
  37.1 0.0 copy-start.9
  37.1 53.6 %all_to_all.30 = bf16[32,1,16,2048]{3,2,1,0:T(8,128)(2,1)S(1)} all-to-all(bf16[32,1,16,2048]{3,2,1,0:T(8,128)(2,1)} %bitcast.113), channel_id=1, replica_groups=mesh['sp'=16,'tp'=2] {'sp','tp'}, dimensions={0} | all-to-all | bytes 4194304 | tf_op jit(solution)/shard_map/all_to_all | solution.py:96
  90.6 0.0 copy-start.3
  90.6 1.3 copy-done.3
  91.9 0.0 copy-done.9
  91.9 2.3 %fusion.7 = f32[512,512]{1,0:T(8,128)} fusion(bf16[512,2048]{1,0:T(8,128)(2,1)S(1)} %bitcast.117, bf16[1,2048,512]{2,1,0:T(8,128)(2,1)S(1)} %copy-done.9), kind=kOutput, calls=%fused_computation.42 | convolution fusion | flops 1073741824 | bytes 5242880 | tf_op jit(solution)/shard_map/dot_general | solution.py:98
  94.2 0.0 copy-done
  94.2 6.3 %convolution_convert_fusion = bf16[512,2048]{1,0:T(8,128)(2,1)} fusion(bf16[1,512,2048]{2,1,0:T(8,128)(2,1)S(1)} %copy-done, bf16[512,2048]{1,0:T(8,128)(2,1)} %bitcast.118, bf16[1,2048,512]{2,1,0:T(8,128)(2,1)} %param.29, f32[512,512]{1,0:T(8,128)} %fusion.7), kind=kOutput, calls=%fused_computation.3 | convolution fusion | flops 2150105088 | bytes 9437184 | tf_op jit(solution)/shard_map/dot_general | solution.py:101
  100.5 0.0 copy-start.8
  100.5 4.0 %all-to-all-start.2 = ((bf16[32,1,16,2048]{3,2,1,0:T(8,128)(2,1)}), bf16[32,1,16,2048]{3,2,1,0:T(8,128)(2,1)}, u32[]{:S(2)}, u32[]{:S(2)}) async-start(bf16[32,1,16,2048]{3,2,1,0:T(8,128)(2,1)} %bitcast.116), calls=%async_computation.2 | async-start | bytes 4194304 | tf_op jit(solution)/shard_map/all_to_all | solution.py:105
  104.5 0.0 copy-done.8
  104.5 0.0 copy-done.1
  104.5 2.0 %fusion.65 = f32[128,512]{1,0:T(8,128)S(1)} fusion(bf16[128,2048]{1,0:T(8,128)(2,1)S(1)} %multiply_convert_fusion, bf16[2048,512]{1,0:T(8,128)(2,1)} %param.31), kind=kOutput, calls=%fused_computation.198 | convolution fusion | flops 268435456 | bytes 2883584 | tf_op jit(solution)/shard_map/dot_general | solution.py:91
  106.5 46.6 %all-to-all-done.2 = bf16[32,1,16,2048]{3,2,1,0:T(8,128)(2,1)} async-done(((bf16[32,1,16,2048]{3,2,1,0:T(8,128)(2,1)}), bf16[32,1,16,2048]{3,2,1,0:T(8,128)(2,1)}, u32[]{:S(2)}, u32[]{:S(2)}) %all-to-all-start.2) | async-done | bytes 2097184 | tf_op jit(solution)/shard_map/all_to_all | solution.py:105
  153.1 5.2 %gather_fusion.1 = bf16[256,2048]{1,0:T(8,128)(2,1)} fusion(bf16[512,2048]{1,0:T(8,128)(2,1)} %bitcast.46, s32[1024]{0:T(1024)S(1)} %pad_clamp_fusion), kind=kCustom, calls=%fused_computation.1 | custom fusion | bytes 2098176 | tf_op jit(solution)/shard_map/gather | solution.py:108
  158.3 1.7 %reshape.130 = bf16[128,2,2048]{2,1,0:T(2,128)(2,1)S(1)} reshape(bf16[256,2048]{1,0:T(8,128)(2,1)} %gather_fusion.1) | data formatting | bytes 2097152 | tf_op jit(solution)/shard_map/reshape | solution.py:108
  160.1 2.5 %fusion.64 = (bf16[128,1,2048]{2,1,0:T(2,128)(2,1)}, bf16[128,1,2048]{2,1,0:T(2,128)(2,1)}) fusion(bf16[128,2,2048]{2,1,0:T(2,128)(2,1)S(1)} %reshape.130), kind=kLoop, calls=%fused_computation.197 | loop fusion | bytes 2097152 | tf_op jit(solution)/shard_map/slice | solution.py:113
  162.6 5.4 %fusion.3 = bf16[128,2048]{1,0:T(8,128)(2,1)} fusion(f32[128,2048]{1,0:T(8,128)} %copy-done.2, bf16[512,2048]{1,0:T(8,128)(2,1)} %param.33, bf16[128,2048]{1,0:T(8,128)(2,1)} %copy-done.1, bf16[2048,512]{1,0:T(8,128)(2,1)} %param.32, bf16[128,1,2048]{2,1,0:T(2,128)(2,1)} %get-tuple-element.6, bf16[128,1,2048]{2,1,0:T(2,128)(2,1)} %get-tuple-element.5, ...), kind=kOutput, calls=%fused_computation.38 | convolution fusion | flops 539361280 | bytes 7603200 | tf_op jit(solution)/shard_map/dot_general | solution.py:94
  (15 shorter events, 0.2 us)
Async XLA Ops:
  0.0 94.2 %copy-start = (bf16[1,512,2048]{2,1,0:T(8,128)(2,1)S(1)}, bf16[1,512,2048]{2,1,0:T(8,128)(2,1)}, u32[]{:S(2)}) copy-start(bf16[1,512,2048]{2,1,0:T(8,128)(2,1)} %param.30) | copy-start | bytes 6291460
  0.9 15.9 %collective-permute-start = (s32[30]{0:T(128)S(1)}, s32[30]{0:T(128)S(1)}, u32[]{:S(2)}, u32[]{:S(2)}) collective-permute-start(s32[30]{0:T(128)S(1)} %slice.297), channel_id=1, source_target_pairs={{0,2},{2,4},{4,6},{6,8},{8,10},{10,12},{12,14},{14,16},{16,18},{18... | collective-permute-start | bytes 368 | tf_op jit(solution)/shard_map/ppermute | solution.py:15
  7.0 12.2 %collective-permute-start.1 = (bf16[30,512]{1,0:T(8,128)(2,1)S(1)}, bf16[30,512]{1,0:T(8,128)(2,1)S(1)}, u32[]{:S(2)}, u32[]{:S(2)}) collective-permute-start(bf16[30,512]{1,0:T(8,128)(2,1)S(1)} %slice.400), channel_id=1, source_target_pairs={{0,2},{2,4},{4,6},{6,8},{8,10},{10,12},{12,14},{14,16},{16,18},{18... | collective-permute-start | bytes 92168 | tf_op jit(solution)/shard_map/ppermute | solution.py:15
  23.2 1.9 %copy-start.6 = (f32[512]{0:T(512)S(1)}, f32[512]{0:T(512)}, u32[]{:S(2)}) copy-start(f32[512]{0:T(512)} %param.22) | copy-start | bytes 6148
  23.2 1.9 %copy-start.7 = (f32[512]{0:T(512)S(1)}, f32[512]{0:T(512)}, u32[]{:S(2)}) copy-start(f32[512]{0:T(512)} %param.21) | copy-start | bytes 6148
  24.4 5.0 %copy-start.4 = (bf16[128,2048]{1,0:T(8,128)(2,1)S(1)}, bf16[128,2048]{1,0:T(8,128)(2,1)}, u32[]{:S(2)}) copy-start(bf16[128,2048]{1,0:T(8,128)(2,1)} %param.24) | copy-start | bytes 1572868
  29.5 4.0 %copy-start.5 = (f32[2048]{0:T(1024)S(1)}, f32[2048]{0:T(1024)}, u32[]{:S(2)}) copy-start(f32[2048]{0:T(1024)} %param.25) | copy-start | bytes 24580
  32.5 1.0 copy-start.2
  33.6 70.8 %copy-start.1 = (bf16[128,2048]{1,0:T(8,128)(2,1)}, bf16[128,2048]{1,0:T(8,128)(2,1)S(1)}, u32[]{:S(2)}) copy-start(bf16[128,2048]{1,0:T(8,128)(2,1)S(1)} %multiply_convert_fusion) | copy-start | bytes 1572868
  37.1 54.9 %copy-start.9 = (bf16[1,2048,512]{2,1,0:T(8,128)(2,1)S(1)}, bf16[1,2048,512]{2,1,0:T(8,128)(2,1)}, u32[]{:S(2)}) copy-start(bf16[1,2048,512]{2,1,0:T(8,128)(2,1)} %param.28) | copy-start | bytes 6291460
  90.6 1.3 copy-start.3
  100.5 4.0 %copy-start.8 = (f32[128,2]{0,1:T(2,128)S(1)}, f32[128,2]{0,1:T(2,128)}, u32[]{:S(2)}) copy-start(f32[128,2]{0,1:T(2,128)} %param.27) | copy-start | bytes 3076
  100.5 52.6 %all-to-all-start.2 = ((bf16[32,1,16,2048]{3,2,1,0:T(8,128)(2,1)}), bf16[32,1,16,2048]{3,2,1,0:T(8,128)(2,1)}, u32[]{:S(2)}, u32[]{:S(2)}) async-start(bf16[32,1,16,2048]{3,2,1,0:T(8,128)(2,1)} %bitcast.116), calls=%async_computation.2 | async-start | bytes 4194304 | tf_op jit(solution)/shard_map/all_to_all | solution.py:105
where the time goes:
time: 169 us; the launch traced here: 168 us
  blocking collectives  57.5 us (34%)
  waiting for transfers between devices  46.6 us (28%)
  local copies, waits for them, and re-layouts  20 us (12%)
  matrix products  19 us (11%)
  other arithmetic  12.3 us (7%)
  starting transfers between devices  12.2 us (7%)
    all_to_all x1, blocking collectives, per_device(): lax.all_to_all(parcel, ('sp', 'tp'), split_axis=0, concat_axis=0, tiled=T...  53.6 us
    all_to_all x1, waiting for transfers between devices, per_device(): lax.all_to_all(jnp.stack(results, axis=1), ('sp', 'tp'), split_axis=0, co...  46.6 us
    ppermute x2, starting transfers between devices, from_behind(): return lax.ppermute(x, axis, pairs)  8.26 us
    dot_general x1, matrix products, per_device(): jnp.dot(hidden, expert_down[0], preferred_element_type=jnp.float32)  6.28 us
    dot_general x1, matrix products, per_device(): jnp.dot(shared_hidden, shared_down, preferred_element_type=jnp.float32)  5.43 us
    gather x1, local copies, waits for them, and re-layouts, per_device(): returned.reshape(experts * capacity, model_width)[target]  5.21 us
    add x1, other arithmetic, per_device(): conv_sum = conv_sum + jnp.where(same_doc, tap_term, 0.0)  4.03 us
    all_to_all x1, starting transfers between devices, per_device(): lax.all_to_all(jnp.stack(results, axis=1), ('sp', 'tp'), split_axis=0, co...  3.96 us
  transfers between devices with their start and end apart: 3, of which 1 were waited for; matrix products, arithmetic and copies ran while one was open for 7% of the time, Pallas kernels for 0%

commit v1 on v0

--- a/solution.py
+++ b/solution.py
@@ -1,6 +1,10 @@
+import functools
+
 import jax
 import jax.numpy as jnp
 from jax import lax
+from jax.experimental import pallas as pl
+from jax.experimental.pallas import tpu as pltpu
 from jax.sharding import PartitionSpec as P
 
 GROUPS = 8
@@ -116,9 +120,461 @@
     return (stream_wide + shared_out + routed).astype(jnp.bfloat16)
 
 
+F32 = jnp.float32
+BF16 = jnp.bfloat16
+MESH_ID = pl.DeviceIdType.MESH
+HALO = 32
+CHUNK = 32
+
+
+def flip(index, bits):
+    out, weight = index, 1
+    while weight <= bits:
+        if (bits // weight) % 2:
+            out = out + weight * (1 - 2 * ((index // weight) % 2))
+        weight *= 2
+    return out
+
+
+def silu(v):
+    return v / (1.0 + jnp.exp(-v))
+
+
+def fused_kernel(
+    n_sp,
+    n_tp,
+    capacity,
+    value_ref,
+    gate_ref,
+    taps_ref,
+    ids_ref,
+    gain_ref,
+    shift_ref,
+    resid_ref,
+    ngain_ref,
+    routes_ref,
+    routes_t_ref,
+    weight_ref,
+    conv_out_hbm,
+    eg_hbm,
+    eu_hbm,
+    ed_hbm,
+    sg_hbm,
+    su_hbm,
+    sd_hbm,
+    out_ref,
+    glu_ext,
+    ids_ext,
+    tap_rows,
+    halo_send,
+    halo_recv,
+    act,
+    act_recv,
+    normed_ref,
+    base_ref,
+    send_buf,
+    arrived,
+    result,
+    returned,
+    conv_out,
+    eg,
+    eu,
+    ed,
+    sg,
+    su,
+    sd,
+    w_sem,
+    halo_sem,
+    act_sem,
+    out_send,
+    out_recv,
+    back_send,
+    back_recv,
+    own_sem,
+):
+    n = n_sp * n_tp
+    sp, tp = lax.axis_index("sp"), lax.axis_index("tp")
+    me = sp * n_tp + tp
+    rows, channels = value_ref.shape
+    tokens, model = resid_ref.shape
+    width = taps_ref.shape[0]
+    group = glu_ext.shape[2]
+    groups = channels // group
+
+    def place(index):
+        return (index // n_tp, index % n_tp)
+
+    loads = [
+        pltpu.make_async_copy(a, b, w_sem.at[i])
+        for i, (a, b) in enumerate(
+            [
+                (conv_out_hbm, conv_out),
+                (sg_hbm, sg),
+                (su_hbm, su),
+                (sd_hbm, sd),
+                (eg_hbm, eg),
+                (eu_hbm, eu),
+                (ed_hbm, ed),
+            ]
+        )
+    ]
+    for load in loads:
+        load.start()
+
+    barrier = pltpu.get_barrier_semaphore()
+    for j in range(1, n):
+        pl.semaphore_signal(barrier, inc=1, device_id=place(flip(me, j)), device_id_type=MESH_ID)
+
+    glu = (value_ref[...].astype(F32) * jax.nn.sigmoid(gate_ref[...].astype(F32))).astype(BF16)
+    halo_send[...] = glu[rows - HALO :, :]
+    for g in range(groups):
+        glu_ext[g, pl.ds(HALO, rows), :] = glu[:, g * group : (g + 1) * group].astype(F32)
+    ids_ext[pl.ds(HALO, rows), :] = ids_ref[...]
+    tap_rows[pl.ds(0, width), :] = taps_ref[...].astype(F32)
+
+    pl.semaphore_wait(barrier, n - 1)
+
+    halo_copies = [
+        pltpu.make_async_remote_copy(
+            src_ref=halo_send,
+            dst_ref=halo_recv,
+            send_sem=halo_sem.at[0],
+            recv_sem=halo_sem.at[1],
+            device_id=(sp + 1, tp),
+            device_id_type=MESH_ID,
+        ),
+        pltpu.make_async_remote_copy(
+            src_ref=ids_ref.at[pl.ds(rows - HALO, HALO)],
+            dst_ref=ids_ext.at[pl.ds(0, HALO)],
+            send_sem=halo_sem.at[2],
+            recv_sem=halo_sem.at[3],
+            device_id=(sp + 1, tp),
+            device_id_type=MESH_ID,
+        ),
+    ]
+
+    @pl.when(sp < n_sp - 1)
+    def _():
+        for copy in halo_copies:
+            copy.start()
+
+    @pl.when(sp == 0)
+    def _():
+        glu_ext[:, pl.ds(0, HALO), :] = jnp.zeros((groups, HALO, group), F32)
+        ids_ext[pl.ds(0, HALO), :] = jnp.full((HALO, ids_ext.shape[1]), -1, jnp.int32)
+
+    slots = n * capacity
+    expert_lane = lax.broadcasted_iota(jnp.int32, (tokens, n), 1)
+    member = (
+        (routes_ref[:, 0:1] == expert_lane).astype(F32)
+        + (routes_ref[:, 1:2] == expert_lane).astype(F32)
+    ).astype(BF16)
+    tri_r = lax.broadcasted_iota(jnp.int32, (tokens, tokens), 0)
+    tri_c = lax.broadcasted_iota(jnp.int32, (tokens, tokens), 1)
+    slot_of = jnp.dot((tri_c < tri_r).astype(F32).astype(BF16), member, preferred_element_type=F32)
+    spread = (
+        (
+            lax.broadcasted_iota(jnp.int32, (n, slots), 1) // capacity
+            == lax.broadcasted_iota(jnp.int32, (n, slots), 0)
+        )
+        .astype(F32)
+        .astype(BF16)
+    )
+    slot_wide = jnp.dot(slot_of.astype(BF16), spread, preferred_element_type=F32)
+    lane = lax.broadcasted_iota(jnp.int32, (tokens, slots), 1)
+    lane_expert = lane // capacity
+    right_slot = slot_wide == (lane % capacity).astype(F32)
+    weights = jnp.where(lane_expert == routes_ref[:, 0:1], weight_ref[:, 0:1], 0.0) + jnp.where(
+        lane_expert == routes_ref[:, 1:2], weight_ref[:, 1:2], 0.0
+    )
+    weights = jnp.where(right_slot, weights, 0.0)
+    w_high = weights.astype(BF16)
+    w_low = (weights - w_high.astype(F32)).astype(BF16)
+
+    expert_row = lax.broadcasted_iota(jnp.int32, (n, tokens), 0)
+    member_t = (
+        (routes_t_ref[0:1, :] == expert_row).astype(F32)
+        + (routes_t_ref[1:2, :] == expert_row).astype(F32)
+    ).astype(BF16)
+    slot_t = jnp.dot(member_t, (tri_r < tri_c).astype(F32).astype(BF16), preferred_element_type=F32)
+    spread_t = (
+        (
+            lax.broadcasted_iota(jnp.int32, (slots, n), 0) // capacity
+            == lax.broadcasted_iota(jnp.int32, (slots, n), 1)
+        )
+        .astype(F32)
+        .astype(BF16)
+    )
+    slot_tall = jnp.dot(spread_t, slot_t.astype(BF16), preferred_element_type=F32)
+    member_tall = jnp.dot(spread_t, member_t, preferred_element_type=F32)
+    row_slot = (lax.broadcasted_iota(jnp.int32, (slots, tokens), 0) % capacity).astype(F32)
+    pick = jnp.where(slot_tall == row_slot, member_tall, 0.0).astype(BF16)
+
+    @pl.when(sp > 0)
+    def _():
+        for copy in halo_copies:
+            copy.wait_recv()
+        for g in range(groups):
+            glu_ext[g, pl.ds(0, HALO), :] = halo_recv[:, g * group : (g + 1) * group].astype(F32)
+
+    @pl.when(sp < n_sp - 1)
+    def _():
+        for copy in halo_copies:
+            copy.wait_send()
+
+    def conv_block(start):
+        def body(i, carry):
+            r = pl.multiple_of(start + i * CHUNK, CHUNK)
+            mine = ids_ref[pl.ds(r, CHUNK), :]
+            sums = [jnp.zeros((CHUNK, group), F32) for _ in range(groups)]
+            for tap in range(width):
+                off = HALO - width + 1 + tap
+                same = ids_ext[pl.ds(r + off, CHUNK), :] == mine
+                for g in range(groups):
+                    term = (
+                        tap_rows[tap : tap + 1, g * group : (g + 1) * group]
+                        * glu_ext[g, pl.ds(r + off, CHUNK), :]
+                    )
+                    sums[g] = sums[g] + jnp.where(same, term, 0.0)
+            for g in range(groups):
+                cols = slice(g * group, (g + 1) * group)
+                centered = sums[g] - jnp.mean(sums[g], axis=-1, keepdims=True)
+                var = jnp.mean(centered * centered, axis=-1, keepdims=True)
+                v = centered * lax.rsqrt(var + epsilon) * gain_ref[:, cols] + shift_ref[:, cols]
+                act[pl.ds(r, CHUNK), cols] = silu(v).astype(BF16)
+            return carry
+
+        lax.fori_loop(0, tokens // CHUNK, body, 0)
+
+    other = (tp + 1) % n_tp
+    theirs = pl.multiple_of(other * tokens, tokens)
+    mine_at = pl.multiple_of(tp * tokens, tokens)
+    conv_block(theirs)
+    act_copy = pltpu.make_async_remote_copy(
+        src_ref=act.at[pl.ds(theirs, tokens)],
+        dst_ref=act_recv,
+        send_sem=act_sem.at[0],
+        recv_sem=act_sem.at[1],
+        device_id=(sp, other),
+        device_id_type=MESH_ID,
+    )
+    act_copy.start()
+    conv_block(mine_at)
+    loads[0].wait()
+    half = channels
+    projected = jnp.dot(
+        act[pl.ds(mine_at, tokens), :],
+        conv_out[pl.ds(pl.multiple_of(tp * half, half), half), :],
+        preferred_element_type=F32,
+    )
+    act_copy.wait()
+    projected = projected + jnp.dot(
+        act_recv[...],
+        conv_out[pl.ds(pl.multiple_of(other * half, half), half), :],
+        preferred_element_type=F32,
+    )
+    stream = (resid_ref[...].astype(F32) + projected).astype(BF16).astype(F32)
+    base_ref[...] = stream
+    normed = (
+        stream
+        * lax.rsqrt(jnp.mean(stream * stream, axis=-1, keepdims=True) + epsilon)
+        * ngain_ref[...]
+    ).astype(BF16)
+    normed_ref[...] = normed
+
+    batches = BATCHES
+    per = n // batches
+    block = per * capacity
+
+    def outgoing(index, peer):
+        return pltpu.make_async_remote_copy(
+            src_ref=send_buf.at[pl.ds(pl.multiple_of(peer * capacity, capacity), capacity)],
+            dst_ref=arrived.at[pl.ds(pl.multiple_of(me * capacity, capacity), capacity)],
+            send_sem=out_send.at[index],
+            recv_sem=out_recv.at[index],
+            device_id=place(peer),
+            device_id_type=MESH_ID,
+        )
+
+    def incoming(index, peer):
+        return pltpu.make_async_remote_copy(
+            src_ref=send_buf.at[pl.ds(pl.multiple_of(me * capacity, capacity), capacity)],
+            dst_ref=arrived.at[pl.ds(pl.multiple_of(peer * capacity, capacity), capacity)],
+            send_sem=out_send.at[index],
+            recv_sem=out_recv.at[index],
+            device_id=place(peer),
+            device_id_type=MESH_ID,
+        )
+
+    def homeward(index, peer):
+        return pltpu.make_async_remote_copy(
+            src_ref=result.at[pl.ds(pl.multiple_of(peer * capacity, capacity), capacity)],
+            dst_ref=returned.at[pl.ds(pl.multiple_of(me * capacity, capacity), capacity)],
+            send_sem=back_send.at[index],
+            recv_sem=back_recv.at[index],
+            device_id=place(peer),
+            device_id_type=MESH_ID,
+        )
+
+    def coming_home(index, peer):
+        return pltpu.make_async_remote_copy(
+            src_ref=result.at[pl.ds(pl.multiple_of(me * capacity, capacity), capacity)],
+            dst_ref=returned.at[pl.ds(pl.multiple_of(peer * capacity, capacity), capacity)],
+            send_sem=back_send.at[index],
+            recv_sem=back_recv.at[index],
+            device_id=place(peer),
+            device_id_type=MESH_ID,
+        )
+
+    send_buf[...] = jnp.dot(pick, normed, preferred_element_type=F32).astype(BF16)
+    for j in range(n - 1, 0, -1):
+        outgoing(j, flip(me, j)).start()
+    own = pl.ds(pl.multiple_of(me * capacity, capacity), capacity)
+    arrived[own, :] = send_buf[own, :]
+
+    for load in loads[1:4]:
+        load.wait()
+    shared = (
+        silu(jnp.dot(normed_ref[...], sg[...], preferred_element_type=F32))
+        * jnp.dot(normed_ref[...], su[...], preferred_element_type=F32)
+    ).astype(BF16)
+    base_ref[...] += jnp.dot(shared, sd[...], preferred_element_type=F32)
+    for load in loads[4:]:
+        load.wait()
+
+    for b in range(batches - 1, -1, -1):
+        for low in range(per - 1, -1, -1):
+            j = b * per + low
+            if j:
+                incoming(j, flip(me, j)).wait_recv()
+        at = pl.ds(pl.multiple_of(flip(me // per, b) * block, block), block)
+        x = arrived[at, :]
+        hidden = (
+            silu(jnp.dot(x, eg[0], preferred_element_type=F32))
+            * jnp.dot(x, eu[0], preferred_element_type=F32)
+        ).astype(BF16)
+        result[at, :] = jnp.dot(hidden, ed[0], preferred_element_type=F32).astype(BF16)
+        for low in range(per - 1, -1, -1):
+            j = b * per + low
+            if j:
+                homeward(j, flip(me, j)).start()
+    returned[own, :] = result[own, :]
+
+    for j in range(n - 1, 0, -1):
+        coming_home(j, flip(me, j)).wait_recv()
+    back = returned[...]
+    routed = jnp.dot(w_high, back, preferred_element_type=F32) + jnp.dot(
+        w_low, back, preferred_element_type=F32
+    )
+    out_ref[...] = (base_ref[...] + routed).astype(BF16)
+    for j in range(n - 1, 0, -1):
+        outgoing(j, flip(me, j)).wait_send()
+        homeward(j, flip(me, j)).wait_send()
+
+
+def fused(
+    conv_value,
+    conv_gate,
+    taps,
+    doc_ids,
+    gn_gain,
+    gn_shift,
+    conv_out,
+    residual,
+    norm_gain,
+    routes,
+    route_weight,
+    expert_gate,
+    expert_up,
+    expert_down,
+    shared_gate,
+    shared_up,
+    shared_down,
+):
+    n_sp, n_tp = lax.axis_size("sp"), lax.axis_size("tp")
+    n = n_sp * n_tp
+    rows, channels = conv_value.shape
+    tokens, model = residual.shape
+    capacity = 2 * tokens * routes.shape[1] // n
+    group = channels * n_tp // GROUPS
+    hidden = expert_gate.shape[2]
+    slots = n * capacity
+    vmem = pl.BlockSpec(memory_space=pltpu.VMEM)
+    hbm = pl.BlockSpec(memory_space=pl.ANY)
+    dma = pltpu.SemaphoreType.DMA
+    ids = jnp.broadcast_to(doc_ids[:, None], (rows, group))
+    return pl.pallas_call(
+        functools.partial(fused_kernel, n_sp, n_tp, capacity),
+        out_shape=jax.ShapeDtypeStruct((tokens, model), BF16),
+        in_specs=[vmem] * 11 + [hbm] * 7,
+        out_specs=vmem,
+        scratch_shapes=[
+            pltpu.VMEM((channels // group, rows + HALO, group), F32),
+            pltpu.VMEM((rows + HALO, group), jnp.int32),
+            pltpu.VMEM((taps.shape[0] + 1, channels), F32),
+            pltpu.VMEM((HALO, channels), BF16),
+            pltpu.VMEM((HALO, channels), BF16),
+            pltpu.VMEM((rows, channels), BF16),
+            pltpu.VMEM((tokens, channels), BF16),
+            pltpu.VMEM((tokens, model), BF16),
+            pltpu.VMEM((tokens, model), F32),
+            pltpu.VMEM((slots, model), BF16),
+            pltpu.VMEM((slots, model), BF16),
+            pltpu.VMEM((slots, model), BF16),
+            pltpu.VMEM((slots, model), BF16),
+            pltpu.VMEM(conv_out.shape, BF16),
+            pltpu.VMEM(expert_gate.shape, BF16),
+            pltpu.VMEM(expert_up.shape, BF16),
+            pltpu.VMEM(expert_down.shape, BF16),
+            pltpu.VMEM(shared_gate.shape, BF16),
+            pltpu.VMEM(shared_up.shape, BF16),
+            pltpu.VMEM(shared_down.shape, BF16),
+            dma((7,)),
+            dma((4,)),
+            dma((2,)),
+            dma((n,)),
+            dma((n,)),
+            dma((n,)),
+            dma((n,)),
+            dma((2,)),
+        ],
+        compiler_params=pltpu.CompilerParams(
+            collective_id=0, has_side_effects=True, vmem_limit_bytes=VMEM_LIMIT
+        ),
+    )(
+        conv_value,
+        conv_gate,
+        taps,
+        ids,
+        gn_gain[None, :],
+        gn_shift[None, :],
+        residual,
+        norm_gain[None, :],
+        routes,
+        routes.T,
+        route_weight,
+        conv_out,
+        expert_gate,
+        expert_up,
+        expert_down,
+        shared_gate,
+        shared_up,
+        shared_down,
+    )
+
+
+BATCHES = 4
+VMEM_LIMIT = 58 * 1024 * 1024
+
+
+def fits(mesh):
+    n = mesh.size
+    return n & (n - 1) == 0 and n <= 32 and mesh.shape["tp"] == 2
+
+
 def solution(mesh):
     return jax.shard_map(
-        per_device,
+        fused if fits(mesh) else per_device,
         mesh=mesh,
         in_specs=(
             P("sp", "tp"),

time: 169 us -> 124 us (0.73)
  Pallas kernels: 0 us -> 117 us
  blocking collectives: 57.5 us -> 0 us
  waiting for transfers between devices: 46.6 us -> 0 us
  matrix products: 19 us -> 0 us
  local copies, waits for them, and re-layouts: 20 us -> 6.12 us
  other arithmetic: 12.3 us -> 0 us
  starting transfers between devices: 12.2 us -> 0 us
    pallas_call x0 -> x1, Pallas kernels: none -> 117 us  [fused(): pl.pallas_call(functools.partial(fused_kernel, n_sp, n_tp, capacity), out...]
    all_to_all x2 -> x0, blocking collectives: 57.5 us -> none  [the longest x1 53.6 us: per_device(): lax.all_to_all(parcel, ('sp', 'tp'), split_axis=0, concat_axis=0, tiled=T...]
    all_to_all x1 -> x0, waiting for transfers between devices: 46.6 us -> none  [per_device(): lax.all_to_all(jnp.stack(results, axis=1), ('sp', 'tp'), split_axis=0, co...]
    dot_general x5 -> x0, matrix products: 19 us -> none  [the longest x1 6.28 us: per_device(): jnp.dot(hidden, expert_down[0], preferred_element_type=jnp.float32)]
    gather x2 -> x0, local copies, waits for them, and re-layouts: 8.56 us -> none  [the longest x1 5.21 us: per_device(): returned.reshape(experts * capacity, model_width)[target]]
    ppermute x2 -> x0, starting transfers between devices: 8.26 us -> none  [from_behind(): return lax.ppermute(x, axis, pairs)]
    add x1 -> x0, other arithmetic: 4.03 us -> none  [per_device(): conv_sum = conv_sum + jnp.where(same_doc, tap_term, 0.0)]
    all_to_all x1 -> x0, starting transfers between devices: 3.96 us -> none  [per_device(): lax.all_to_all(jnp.stack(results, axis=1), ('sp', 'tp'), split_axis=0, co...]
  transfers between devices with their start and end apart: 3 -> 0, of which waited for: 1 -> 0; matrix products, arithmetic and copies ran while one was open for 7% -> 0% of each run, Pallas kernels for 0% -> 0%
where the time goes in v1:
time: 124 us
  Pallas kernels  117 us (94%)
  local copies, waits for them, and re-layouts  6.12 us (5%)
    pallas_call x1, Pallas kernels, fused(): pl.pallas_call(functools.partial(fused_kernel, n_sp, n_tp, capacity), out...  117 us
    unnamed x3, local copies, waits for them, and re-layouts  4.69 us

profile of v1, /device:TPU:0, one launch (start us, length us, event | category | flops | bytes accessed | tf_op | source)
XLA Modules:
  0.0 123.5 jit_solution(17664559808824011420)
XLA Ops:
  0.0 1.4 %copy.19.weight_ref = f32[128,2]{1,0:T(8,128)} copy(f32[128,2]{0,1:T(2,128)} %param.27) | data formatting | bytes 2048 | tf_op args[10]
  1.4 1.4 %copy.18.routes_ref = s32[128,2]{1,0:T(8,128)} copy(s32[128,2]{0,1:T(2,128)} %param.26) | data formatting | bytes 2048 | tf_op args[9]
  2.8 1.4 %broadcast_in_dim.15.ids_ref = s32[256,128]{1,0:T(8,128)} broadcast(s32[256]{0:T(256)} %param.20), dimensions={0} | broadcast | bytes 132096 | tf_op jit(solution)/shard_map/broadcast_in_dim | solution.py:505
  4.2 117.4 %shard_map.163 = bf16[128,2048]{1,0:T(8,128)(2,1)} custom-call(bf16[256,512]{1,0:T(8,128)(2,1)} %value_ref.1, bf16[256,512]{1,0:T(8,128)(2,1)} %gate_ref.1, bf16[31,512]{1,0:T(8,128)(2,1)} %taps_ref.1, s32[256,128]{1,0:T(8,128)} %broadcast_in_dim.15.ids_ref, f32[1,512]{1,0:T(1,128)} %bitcast.6, f32[1,512]{1,0:T(1,128)} %bitcast.7, ...), custom_call_target="tpu_custom_call" | custom-call | tf_op jit(solution)/shard_map/pallas_call | solution.py:506
  121.6 1.9 %copy.21 = bf16[128,2048]{1,0:T(8,128)(2,1)} copy(bf16[128,2048]{1,0:T(8,128)(2,1)} %shard_map.163) | data formatting | bytes 1048576

commit v2 on v1

--- a/solution.py
+++ b/solution.py
@@ -153,7 +153,6 @@
     resid_ref,
     ngain_ref,
     routes_ref,
-    routes_t_ref,
     weight_ref,
     conv_out_hbm,
     eg_hbm,
@@ -172,10 +171,18 @@
     act_recv,
     normed_ref,
     base_ref,
-    send_buf,
+    far_tokens,
+    far_routes,
+    far_weight,
+    ids_here,
+    send_own,
+    send_far,
     arrived,
     result,
     returned,
+    relayed,
+    part_send,
+    part_recv,
     conv_out,
     eg,
     eu,
@@ -190,7 +197,7 @@
     out_recv,
     back_send,
     back_recv,
-    own_sem,
+    far_sem,
 ):
     n = n_sp * n_tp
     sp, tp = lax.axis_index("sp"), lax.axis_index("tp")
@@ -200,6 +207,9 @@
     width = taps_ref.shape[0]
     group = glu_ext.shape[2]
     groups = channels // group
+
+    near = n // 2
+    far = flip(me, near)
 
     def place(index):
         return (index // n_tp, index % n_tp)
@@ -229,7 +239,11 @@
     halo_send[...] = glu[rows - HALO :, :]
     for g in range(groups):
         glu_ext[g, pl.ds(HALO, rows), :] = glu[:, g * group : (g + 1) * group].astype(F32)
-    ids_ext[pl.ds(HALO, rows), :] = ids_ref[...]
+    for at in range(0, rows, group):
+        row = ids_ref[:, at : at + group].astype(F32)
+        column = jnp.broadcast_to(row, (group, group)).T
+        ids_here[pl.ds(at, group), :] = column
+        ids_ext[pl.ds(HALO + at, group), :] = column
     tap_rows[pl.ds(0, width), :] = taps_ref[...].astype(F32)
 
     pl.semaphore_wait(barrier, n - 1)
@@ -244,7 +258,7 @@
             device_id_type=MESH_ID,
         ),
         pltpu.make_async_remote_copy(
-            src_ref=ids_ref.at[pl.ds(rows - HALO, HALO)],
+            src_ref=ids_here.at[pl.ds(rows - HALO, HALO)],
             dst_ref=ids_ext.at[pl.ds(0, HALO)],
             send_sem=halo_sem.at[2],
             recv_sem=halo_sem.at[3],
@@ -261,54 +275,55 @@
     @pl.when(sp == 0)
     def _():
         glu_ext[:, pl.ds(0, HALO), :] = jnp.zeros((groups, HALO, group), F32)
-        ids_ext[pl.ds(0, HALO), :] = jnp.full((HALO, ids_ext.shape[1]), -1, jnp.int32)
-
-    slots = n * capacity
-    expert_lane = lax.broadcasted_iota(jnp.int32, (tokens, n), 1)
-    member = (
-        (routes_ref[:, 0:1] == expert_lane).astype(F32)
-        + (routes_ref[:, 1:2] == expert_lane).astype(F32)
-    ).astype(BF16)
+        ids_ext[pl.ds(0, HALO), :] = jnp.full((HALO, group), -1.0, F32)
+
+    def to_far(src, dst, index):
+        return pltpu.make_async_remote_copy(
+            src_ref=src,
+            dst_ref=dst,
+            send_sem=far_sem.at[2 * index],
+            recv_sem=far_sem.at[2 * index + 1],
+            device_id=place(far),
+            device_id_type=MESH_ID,
+        )
+
+    routes_copy = to_far(routes_ref, far_routes, 0)
+    weight_copy = to_far(weight_ref, far_weight, 1)
+    routes_copy.start()
+    weight_copy.start()
+
+    slots = near * capacity
+    first = (me // near) * near
     tri_r = lax.broadcasted_iota(jnp.int32, (tokens, tokens), 0)
     tri_c = lax.broadcasted_iota(jnp.int32, (tokens, tokens), 1)
-    slot_of = jnp.dot((tri_c < tri_r).astype(F32).astype(BF16), member, preferred_element_type=F32)
-    spread = (
+    later = (tri_r < tri_c).astype(F32).astype(BF16)
+    spread_t = (
         (
-            lax.broadcasted_iota(jnp.int32, (n, slots), 1) // capacity
-            == lax.broadcasted_iota(jnp.int32, (n, slots), 0)
+            lax.broadcasted_iota(jnp.int32, (slots, near), 0) // capacity
+            == lax.broadcasted_iota(jnp.int32, (slots, near), 1)
         )
         .astype(F32)
         .astype(BF16)
     )
-    slot_wide = jnp.dot(slot_of.astype(BF16), spread, preferred_element_type=F32)
-    lane = lax.broadcasted_iota(jnp.int32, (tokens, slots), 1)
-    lane_expert = lane // capacity
-    right_slot = slot_wide == (lane % capacity).astype(F32)
-    weights = jnp.where(lane_expert == routes_ref[:, 0:1], weight_ref[:, 0:1], 0.0) + jnp.where(
-        lane_expert == routes_ref[:, 1:2], weight_ref[:, 1:2], 0.0
-    )
-    weights = jnp.where(right_slot, weights, 0.0)
-    w_high = weights.astype(BF16)
-    w_low = (weights - w_high.astype(F32)).astype(BF16)
-
-    expert_row = lax.broadcasted_iota(jnp.int32, (n, tokens), 0)
-    member_t = (
-        (routes_t_ref[0:1, :] == expert_row).astype(F32)
-        + (routes_t_ref[1:2, :] == expert_row).astype(F32)
-    ).astype(BF16)
-    slot_t = jnp.dot(member_t, (tri_r < tri_c).astype(F32).astype(BF16), preferred_element_type=F32)
-    spread_t = (
-        (
-            lax.broadcasted_iota(jnp.int32, (slots, n), 0) // capacity
-            == lax.broadcasted_iota(jnp.int32, (slots, n), 1)
-        )
-        .astype(F32)
-        .astype(BF16)
-    )
-    slot_tall = jnp.dot(spread_t, slot_t.astype(BF16), preferred_element_type=F32)
-    member_tall = jnp.dot(spread_t, member_t, preferred_element_type=F32)
     row_slot = (lax.broadcasted_iota(jnp.int32, (slots, tokens), 0) % capacity).astype(F32)
-    pick = jnp.where(slot_tall == row_slot, member_tall, 0.0).astype(BF16)
+    row_expert = first + lax.broadcasted_iota(jnp.int32, (slots, tokens), 0) // capacity
+    expert_row = first + lax.broadcasted_iota(jnp.int32, (near, tokens), 0)
+
+    def tables(routes, weight):
+        member = (
+            (routes[0:1, :] == expert_row).astype(F32)
+            + (routes[1:2, :] == expert_row).astype(F32)
+        ).astype(BF16)
+        slot = jnp.dot(member, later, preferred_element_type=F32).astype(BF16)
+        right = jnp.dot(spread_t, slot, preferred_element_type=F32) == row_slot
+        hit0 = jnp.where(right & (routes[0:1, :] == row_expert), 1.0, 0.0)
+        hit1 = jnp.where(right & (routes[1:2, :] == row_expert), 1.0, 0.0)
+        pick = (hit0 + hit1).astype(BF16)
+        mix = (hit0 * weight[0:1, :] + hit1 * weight[1:2, :]).T
+        high = mix.astype(BF16)
+        return pick, high, (mix - high.astype(F32)).astype(BF16)
+
+    pick, w_high, w_low = tables(routes_ref[...], weight_ref[...])
 
     @pl.when(sp > 0)
     def _():
@@ -325,7 +340,7 @@
     def conv_block(start):
         def body(i, carry):
             r = pl.multiple_of(start + i * CHUNK, CHUNK)
-            mine = ids_ref[pl.ds(r, CHUNK), :]
+            mine = ids_here[pl.ds(r, CHUNK), :]
             sums = [jnp.zeros((CHUNK, group), F32) for _ in range(groups)]
             for tap in range(width):
                 off = HALO - width + 1 + tap
@@ -382,55 +397,54 @@
     ).astype(BF16)
     normed_ref[...] = normed
 
-    batches = BATCHES
-    per = n // batches
+    per = near // 2
     block = per * capacity
 
-    def outgoing(index, peer):
+    def piece(index):
+        return pl.ds(pl.multiple_of(index * capacity, capacity), capacity)
+
+    def exchange(src, dst, sems, index, peer):
         return pltpu.make_async_remote_copy(
-            src_ref=send_buf.at[pl.ds(pl.multiple_of(peer * capacity, capacity), capacity)],
-            dst_ref=arrived.at[pl.ds(pl.multiple_of(me * capacity, capacity), capacity)],
-            send_sem=out_send.at[index],
-            recv_sem=out_recv.at[index],
+            src_ref=src,
+            dst_ref=dst,
+            send_sem=sems[0].at[index],
+            recv_sem=sems[1].at[index],
             device_id=place(peer),
             device_id_type=MESH_ID,
         )
 
-    def incoming(index, peer):
-        return pltpu.make_async_remote_copy(
-            src_ref=send_buf.at[pl.ds(pl.multiple_of(me * capacity, capacity), capacity)],
-            dst_ref=arrived.at[pl.ds(pl.multiple_of(peer * capacity, capacity), capacity)],
-            send_sem=out_send.at[index],
-            recv_sem=out_recv.at[index],
-            device_id=place(peer),
-            device_id_type=MESH_ID,
+    out_sems, back_sems = (out_send, out_recv), (back_send, back_recv)
+    here = me % near
+
+    def own_out(k):
+        peer = flip(me, k)
+        return exchange(send_own.at[piece(peer % near)], arrived.at[piece(me)], out_sems, k, peer)
+
+    def far_out(k):
+        peer = flip(me, k)
+        return exchange(
+            send_far.at[piece(peer % near)], arrived.at[piece(far)], out_sems, near + k, peer
         )
 
-    def homeward(index, peer):
-        return pltpu.make_async_remote_copy(
-            src_ref=result.at[pl.ds(pl.multiple_of(peer * capacity, capacity), capacity)],
-            dst_ref=returned.at[pl.ds(pl.multiple_of(me * capacity, capacity), capacity)],
-            send_sem=back_send.at[index],
-            recv_sem=back_recv.at[index],
-            device_id=place(peer),
-            device_id_type=MESH_ID,
+    def own_back(k):
+        peer = flip(me, k)
+        return exchange(result.at[piece(peer)], returned.at[piece(here)], back_sems, k, peer)
+
+    def far_back(k):
+        peer, source = flip(me, k), flip(me, near + k)
+        return exchange(
+            result.at[piece(source)], relayed.at[piece(here)], back_sems, near + k, peer
         )
 
-    def coming_home(index, peer):
-        return pltpu.make_async_remote_copy(
-            src_ref=result.at[pl.ds(pl.multiple_of(me * capacity, capacity), capacity)],
-            dst_ref=returned.at[pl.ds(pl.multiple_of(peer * capacity, capacity), capacity)],
-            send_sem=back_send.at[index],
-            recv_sem=back_recv.at[index],
-            device_id=place(peer),
-            device_id_type=MESH_ID,
-        )
-
-    send_buf[...] = jnp.dot(pick, normed, preferred_element_type=F32).astype(BF16)
-    for j in range(n - 1, 0, -1):
-        outgoing(j, flip(me, j)).start()
-    own = pl.ds(pl.multiple_of(me * capacity, capacity), capacity)
-    arrived[own, :] = send_buf[own, :]
+    token_copy = to_far(normed_ref, far_tokens, 2)
+    token_copy.start()
+    send_own[...] = jnp.dot(pick, normed_ref[...], preferred_element_type=F32).astype(BF16)
+    for k in range(near - 1, 0, -1):
+        own_out(k).start()
+    arrived[piece(me), :] = send_own[piece(here), :]
+    routes_copy.wait()
+    weight_copy.wait()
+    far_pick, far_high, far_low = tables(far_routes[...], far_weight[...])
 
     for load in loads[1:4]:
         load.wait()
@@ -442,11 +456,11 @@
     for load in loads[4:]:
         load.wait()
 
-    for b in range(batches - 1, -1, -1):
-        for low in range(per - 1, -1, -1):
+    def experts(b):
+        for low in range(per):
             j = b * per + low
-            if j:
-                incoming(j, flip(me, j)).wait_recv()
+            if j % near:
+                (own_out(j) if j < near else far_out(j - near)).wait_recv()
         at = pl.ds(pl.multiple_of(flip(me // per, b) * block, block), block)
         x = arrived[at, :]
         hidden = (
@@ -454,22 +468,53 @@
             * jnp.dot(x, eu[0], preferred_element_type=F32)
         ).astype(BF16)
         result[at, :] = jnp.dot(hidden, ed[0], preferred_element_type=F32).astype(BF16)
-        for low in range(per - 1, -1, -1):
-            j = b * per + low
-            if j:
-                homeward(j, flip(me, j)).start()
-    returned[own, :] = result[own, :]
-
-    for j in range(n - 1, 0, -1):
-        coming_home(j, flip(me, j)).wait_recv()
+
+    token_copy.wait_recv()
+    send_far[...] = jnp.dot(far_pick, far_tokens[...], preferred_element_type=F32).astype(BF16)
+    for k in range(near - 1, 0, -1):
+        far_out(k).start()
+    arrived[piece(far), :] = send_far[piece(here), :]
+
+    experts(0)
+    for k in range(per - 1, 0, -1):
+        own_back(k).start()
+    returned[piece(here), :] = result[piece(me), :]
+    experts(1)
+    experts(2)
+    for k in range(per - 1, 0, -1):
+        far_back(k).start()
+    relayed[piece(here), :] = result[piece(far), :]
+    experts(3)
+    for k in range(near - 1, per - 1, -1):
+        far_back(k).start()
+
+    for k in range(1, near):
+        far_back(k).wait_recv()
+    back = relayed[...]
+    part_send[...] = (
+        jnp.dot(far_high, back, preferred_element_type=F32)
+        + jnp.dot(far_low, back, preferred_element_type=F32)
+    ).astype(BF16)
+    part_copy = to_far(part_send, part_recv, 3)
+    part_copy.start()
+    for k in range(near - 1, per - 1, -1):
+        own_back(k).start()
+
+    for k in range(1, near):
+        own_back(k).wait_recv()
     back = returned[...]
-    routed = jnp.dot(w_high, back, preferred_element_type=F32) + jnp.dot(
+    base_ref[...] += jnp.dot(w_high, back, preferred_element_type=F32) + jnp.dot(
         w_low, back, preferred_element_type=F32
     )
-    out_ref[...] = (base_ref[...] + routed).astype(BF16)
-    for j in range(n - 1, 0, -1):
-        outgoing(j, flip(me, j)).wait_send()
-        homeward(j, flip(me, j)).wait_send()
+    part_copy.wait_recv()
+    out_ref[...] = (base_ref[...] + part_recv[...].astype(F32)).astype(BF16)
+    for k in range(1, near):
+        own_out(k).wait_send()
+        far_out(k).wait_send()
+        own_back(k).wait_send()
+        far_back(k).wait_send()
+    token_copy.wait_send()
+    part_copy.wait_send()
 
 
 def fused(
@@ -497,20 +542,18 @@
     tokens, model = residual.shape
     capacity = 2 * tokens * routes.shape[1] // n
     group = channels * n_tp // GROUPS
-    hidden = expert_gate.shape[2]
-    slots = n * capacity
+    near_slots = n // 2 * capacity
     vmem = pl.BlockSpec(memory_space=pltpu.VMEM)
     hbm = pl.BlockSpec(memory_space=pl.ANY)
     dma = pltpu.SemaphoreType.DMA
-    ids = jnp.broadcast_to(doc_ids[:, None], (rows, group))
     return pl.pallas_call(
         functools.partial(fused_kernel, n_sp, n_tp, capacity),
         out_shape=jax.ShapeDtypeStruct((tokens, model), BF16),
-        in_specs=[vmem] * 11 + [hbm] * 7,
+        in_specs=[vmem] * 10 + [hbm] * 7,
         out_specs=vmem,
         scratch_shapes=[
             pltpu.VMEM((channels // group, rows + HALO, group), F32),
-            pltpu.VMEM((rows + HALO, group), jnp.int32),
+            pltpu.VMEM((rows + HALO, group), F32),
             pltpu.VMEM((taps.shape[0] + 1, channels), F32),
             pltpu.VMEM((HALO, channels), BF16),
             pltpu.VMEM((HALO, channels), BF16),
@@ -518,10 +561,18 @@
             pltpu.VMEM((tokens, channels), BF16),
             pltpu.VMEM((tokens, model), BF16),
             pltpu.VMEM((tokens, model), F32),
-            pltpu.VMEM((slots, model), BF16),
-            pltpu.VMEM((slots, model), BF16),
-            pltpu.VMEM((slots, model), BF16),
-            pltpu.VMEM((slots, model), BF16),
+            pltpu.VMEM((tokens, model), BF16),
+            pltpu.VMEM((2, tokens), jnp.int32),
+            pltpu.VMEM((2, tokens), F32),
+            pltpu.VMEM((rows, group), F32),
+            pltpu.VMEM((near_slots, model), BF16),
+            pltpu.VMEM((near_slots, model), BF16),
+            pltpu.VMEM((2 * near_slots, model), BF16),
+            pltpu.VMEM((2 * near_slots, model), BF16),
+            pltpu.VMEM((near_slots, model), BF16),
+            pltpu.VMEM((near_slots, model), BF16),
+            pltpu.VMEM((tokens, model), BF16),
+            pltpu.VMEM((tokens, model), BF16),
             pltpu.VMEM(conv_out.shape, BF16),
             pltpu.VMEM(expert_gate.shape, BF16),
             pltpu.VMEM(expert_up.shape, BF16),
@@ -536,7 +587,7 @@
             dma((n,)),
             dma((n,)),
             dma((n,)),
-            dma((2,)),
+            dma((8,)),
         ],
         compiler_params=pltpu.CompilerParams(
             collective_id=0, has_side_effects=True, vmem_limit_bytes=VMEM_LIMIT
@@ -545,14 +596,13 @@
         conv_value,
         conv_gate,
         taps,
-        ids,
+        doc_ids[None, :],
         gn_gain[None, :],
         gn_shift[None, :],
         residual,
         norm_gain[None, :],
-        routes,
         routes.T,
-        route_weight,
+        route_weight.T,
         conv_out,
         expert_gate,
         expert_up,
@@ -563,7 +613,6 @@
     )
 
 
-BATCHES = 4
 VMEM_LIMIT = 58 * 1024 * 1024
 
 

time: 124 us -> 98.2 us (0.79)
  Pallas kernels: 117 us -> 96.1 us
  local copies, waits for them, and re-layouts: 6.12 us -> 1.88 us
    pallas_call x1, Pallas kernels: 117 us -> 96.1 us  [fused(): pl.pallas_call(functools.partial(fused_kernel, n_sp, n_tp, capacity), out...]
    unnamed x3 -> x1, local copies, waits for them, and re-layouts: 4.69 us -> 1.88 us
    broadcast_in_dim x1 -> x0, local copies, waits for them, and re-layouts: 1.43 us -> none  [fused(): ids = jnp.broadcast_to(doc_ids[:, None], (rows, group))]
where the time goes in v2:
time: 98.2 us; the launch traced here: 98 us
  Pallas kernels  96.1 us (98%)
  local copies, waits for them, and re-layouts  1.88 us (2%)
    pallas_call x1, Pallas kernels, fused(): pl.pallas_call(functools.partial(fused_kernel, n_sp, n_tp, capacity), out...  96.1 us

profile of v2, /device:TPU:0, one launch (start us, length us, event | category | flops | bytes accessed | tf_op | source)
XLA Modules:
  0.0 98.0 jit_solution(6134046307741346892)
XLA Ops:
  0.0 96.1 %shard_map.163 = bf16[128,2048]{1,0:T(8,128)(2,1)} custom-call(bf16[256,512]{1,0:T(8,128)(2,1)} %value_ref.1, bf16[256,512]{1,0:T(8,128)(2,1)} %gate_ref.1, bf16[31,512]{1,0:T(8,128)(2,1)} %taps_ref.1, s32[1,256]{1,0:T(1,128)} %bitcast.9, f32[1,512]{1,0:T(1,128)} %bitcast.7, f32[1,512]{1,0:T(1,128)} %bitcast.8, bf16[128,2048]{1,0:T(8,128)(2,1)} %resid_ref.1, ...), custom_call_target="tpu_custom_call" | custom-call | tf_op jit(solution)/shard_map/pallas_call | solution.py:549
  96.1 1.9 %copy.19 = bf16[128,2048]{1,0:T(8,128)(2,1)} copy(bf16[128,2048]{1,0:T(8,128)(2,1)} %shard_map.163) | data formatting | bytes 1048576
